TPU v7x, 128 devices: a whole 4x4x4 slice. The times are simulated.
128 devices in a mesh: ep: 128 (over z, y, x, core).
Axes of the slice: x: 4, y: 4, z: 4, core: 2. Of those that a mesh axis runs over, the one named last changes fastest.
Arguments:
- tokens: bfloat16 [1024, 2048], P('ep'), may hold values from -6 to 6
- cache_keys: bfloat16 [1024, 1024, 128], P('ep'), may hold values from -80 to 80
- cache_values: bfloat16 [1024, 1024, 128], P('ep'), may hold values from -6 to 6
- cum_gates: float32 [1024, 1024, 2], P('ep'), may hold values from -1024 to 0, as said below
- lengths: int32 [1024], P('ep'), may hold values from 128 to 1024
- query_weight: bfloat16 [2048, 2048], replicated, may hold values from -0.125 to 0.125
- key_weight: bfloat16 [2048, 128], replicated, may hold values from -0.125 to 0.125
- value_weight: bfloat16 [2048, 128], replicated, may hold values from -0.125 to 0.125
- forget_weight: bfloat16 [2048, 2], replicated, may hold values from -0.125 to 0.125
- out_weight: bfloat16 [2048, 2048], P('ep'), may hold values from -1 to 1
- norm_gain: float32 [2, 2048], replicated, may hold values from 0.1 to 1.9
- norm_bias: float32 [2, 2048], replicated, may hold values from -1 to 1
- dense_gate_weight: bfloat16 [2048, 5632], P(None, 'ep'), may hold values from -0.125 to 0.125
- dense_up_weight: bfloat16 [2048, 5632], P(None, 'ep'), may hold values from -0.125 to 0.125
- dense_down_weight: bfloat16 [5632, 2048], P('ep'), may hold values from -0.078125 to 0.078125
- dense_scale: float32 [2048], replicated, may hold values from 0.2 to 1.5
- expert_gate_weight: bfloat16 [2048, 57344], P(None, 'ep'), may hold values from -0.125 to 0.125
- expert_up_weight: bfloat16 [2048, 57344], P(None, 'ep'), may hold values from -0.125 to 0.125
- expert_down_weight: bfloat16 [57344, 2048], P('ep'), may hold values from -0.0625 to 0.0625
- routes: int32 [1024, 2], replicated, may hold values from 0 to 7, all different within a row; in each aligned block of 8 rows (0 to 7, 8 to 15, ...) at most 3 rows name the same one
- route_weights: float32 [1024, 2], replicated, may hold values from 0.2 to 1
Outputs:
- output: bfloat16 [1024, 2048], P('ep')
Inputs may be any that keep to these rules, and one draw needn't show every extreme that they name: `routes`: each row names 2 different experts; the rows of one device (8 aligned rows) name one expert at most 3 times. `cum_gates`: non-increasing along positions.
All inputs are finite; a program needn't handle non-finite values.
Results may differ from a plain program's by a relative error of at most 0.012.
Values may be sent and summed in bfloat16 or wider, within the bound.
No kernel may reach another device: no remote copies, remote signals or barrier semaphores. Data moves between devices by JAX's collectives and lax.ppermute only.
A program may use at most 128 MiB of HBM per device.

v0:
```python
import jax
import jax.numpy as jnp
from jax import lax
from jax.sharding import PartitionSpec as P

EXPERTS = 8
TOP = 2
CAP = 3


residual_scale = 1.4142135
norm_eps = 1e-05


def partner_2(block, axis, stride):
    count = lax.axis_size(axis)
    route = []
    for low in range(count):
        high = low | 1 << stride
        if high != low and high < count:
            route += [(low, high), (high, low)]
    return lax.ppermute(block, axis, route)


def layer_norm(values, gain_row, shift_row):
    centre = jnp.mean(values, axis=-1, keepdims=True)
    centred = values - centre
    spread = jnp.mean(centred * centred, axis=-1, keepdims=True)
    return (centred * lax.rsqrt(spread + norm_eps) * gain_row + shift_row).astype(jnp.bfloat16)


def attend(
    queries, cached_keys, cached_values, gate_sums, length_row, fresh_key, fresh_value, fresh_gate
):
    amount = queries.shape[0]
    cache_len = cached_keys.shape[1]
    kv_count = fresh_gate.shape[1]
    head_dim = fresh_key.shape[1] // kv_count
    grouped = queries.shape[1] // (kv_count * head_dim)
    query_grid_four = queries.reshape(amount, kv_count, grouped, head_dim)
    key_four = cached_keys.reshape(amount, cache_len, kv_count, head_dim)
    value_four = cached_values.reshape(amount, cache_len, kv_count, head_dim)
    self_key_row = fresh_key.reshape(amount, kv_count, head_dim)
    own_value = fresh_value.astype(jnp.float32).reshape(amount, kv_count, head_dim)
    ratio_value = head_dim ** (-0.5)
    latest = jnp.take_along_axis(gate_sums, (length_row - 1)[:, None, None], axis=1)
    offsets = jnp.transpose(latest - gate_sums + fresh_gate[:, None, :], (0, 2, 1))
    past = jnp.einsum(
        "bkgd,blkd->bkgl", query_grid_four, key_four, preferred_element_type=jnp.float32
    )
    past = past * ratio_value + offsets[:, :, None, :]
    live = jnp.arange(cache_len, dtype=jnp.int32)[None, :] < length_row[:, None]
    past = jnp.where(live[:, None, None, :], past, -jnp.inf)
    self_part = (
        jnp.einsum(
            "rifs,ris->rif", query_grid_four, self_key_row, preferred_element_type=jnp.float32
        )
        * ratio_value
    )
    highest = jnp.maximum(jnp.max(past, axis=-1), self_part)
    past_exp = jnp.exp(past - highest[..., None])
    own_exp = jnp.exp(self_part - highest)
    denominator = jnp.sum(past_exp, axis=-1) + own_exp
    past_weight = (past_exp / denominator[..., None]).astype(jnp.bfloat16)
    own_weight = (own_exp / denominator).astype(jnp.bfloat16)
    mixed = jnp.einsum(
        "bkgl,blkd->bkgd", past_weight, value_four, preferred_element_type=jnp.float32
    )
    mixed = mixed + own_weight.astype(jnp.float32)[..., None] * own_value[:, :, None, :]
    return mixed.reshape(amount, queries.shape[1]).astype(jnp.bfloat16)


def slot_tables(chosen, shares):
    expert_ids = jnp.arange(EXPERTS, dtype=jnp.int32)
    picked = (chosen[..., None] == expert_ids).astype(jnp.int32)
    hits = jnp.sum(picked, axis=2)
    portion = jnp.sum(picked.astype(jnp.float32) * shares[..., None], axis=2)
    ranks = jnp.cumsum(hits, axis=1) - hits
    slot_ids = jnp.arange(CAP, dtype=jnp.int32)
    matched = (hits[..., None] * (ranks[..., None] == slot_ids).astype(jnp.int32)).astype(
        jnp.float32
    )
    return (matched, portion)


def expert_part(inputs, gate_cols, up_cols, down_rows):
    gate_val = jnp.dot(inputs, gate_cols, preferred_element_type=jnp.float32)
    up_val = jnp.dot(inputs, up_cols, preferred_element_type=jnp.float32)
    hidden = (jax.nn.silu(gate_val) * up_val).astype(jnp.bfloat16)
    return jnp.dot(hidden, down_rows, preferred_element_type=jnp.float32).astype(jnp.bfloat16)


def experts_by_exchange(
    settled,
    routes,
    route_weights,
    own_index,
    shards,
    expert_gate_weight,
    expert_up_weight,
    expert_down_weight,
):
    rows_here = settled.shape[0]
    model_width = settled.shape[1]
    own_routes = lax.dynamic_slice_in_dim(routes, own_index * rows_here, rows_here, 0)
    own_shares = lax.dynamic_slice_in_dim(route_weights, own_index * rows_here, rows_here, 0)
    matched, portion = slot_tables(
        own_routes.reshape(1, rows_here, TOP), own_shares.reshape(1, rows_here, TOP)
    )
    matched = matched[0]
    portion = portion[0]
    send_slots = jnp.einsum(
        "sec,sd->ecd", matched.astype(jnp.bfloat16), settled, preferred_element_type=jnp.float32
    ).astype(jnp.bfloat16)
    outgoing = jnp.repeat(send_slots, shards, axis=0)
    received = lax.all_to_all(outgoing, "ep", split_axis=0, concat_axis=0, tiled=True)
    flat = received.reshape(-1, model_width)
    result = expert_part(flat, expert_gate_weight, expert_up_weight, expert_down_weight)
    answered = result.reshape(received.shape)
    returned = lax.all_to_all(answered, "ep", split_axis=0, concat_axis=0, tiled=True)
    summed = jnp.sum(
        returned.reshape(EXPERTS, shards, CAP, model_width).astype(jnp.float32), axis=1
    )
    return jnp.einsum("sec,ecd->sd", matched * portion[..., None], summed)


def local(
    tokens,
    cache_keys,
    cache_values,
    cum_gates,
    lengths,
    query_weight,
    key_weight,
    value_weight,
    forget_weight,
    out_weight,
    norm_gain,
    norm_bias,
    dense_gate_weight,
    dense_up_weight,
    dense_down_weight,
    dense_scale,
    expert_gate_weight,
    expert_up_weight,
    expert_down_weight,
    routes,
    route_weights,
):
    devices = lax.axis_size("ep")
    shards = devices // EXPERTS
    shard_bits = shards.bit_length() - 1
    total_bits = devices.bit_length() - 1
    own_index = lax.axis_index("ep")
    stacked = jnp.stack([dense_gate_weight, dense_up_weight, jnp.transpose(dense_down_weight)])
    for bit in range(shard_bits, total_bits):
        partner = partner_2(stacked, "ep", bit)
        upper = own_index >> bit & 1 == 1
        stacked = jnp.where(
            upper,
            jnp.concatenate([partner, stacked], axis=2),
            jnp.concatenate([stacked, partner], axis=2),
        )
    query = jnp.dot(tokens, query_weight, preferred_element_type=jnp.float32).astype(jnp.bfloat16)
    new_key = jnp.dot(tokens, key_weight, preferred_element_type=jnp.float32).astype(jnp.bfloat16)
    new_value = jnp.dot(tokens, value_weight, preferred_element_type=jnp.float32).astype(
        jnp.bfloat16
    )
    new_gate = jax.nn.log_sigmoid(
        jnp.dot(tokens, forget_weight, preferred_element_type=jnp.float32)
    )
    attended = attend(
        query, cache_keys, cache_values, cum_gates, lengths, new_key, new_value, new_gate
    )
    projected = jnp.dot(
        attended,
        lax.all_gather(out_weight, "ep", axis=0, tiled=True),
        preferred_element_type=jnp.float32,
    )
    settled = layer_norm(
        residual_scale * tokens.astype(jnp.float32) + projected, norm_gain[0], norm_bias[0]
    )
    group_rows = settled
    for bit in range(shard_bits):
        partner_rows = partner_2(group_rows, "ep", bit)
        upper = own_index >> bit & 1 == 1
        group_rows = jnp.where(
            upper,
            jnp.concatenate([partner_rows, group_rows], axis=0),
            jnp.concatenate([group_rows, partner_rows], axis=0),
        )
    dense_gate = jnp.dot(group_rows, stacked[0], preferred_element_type=jnp.float32)
    dense_up = jnp.dot(group_rows, stacked[1], preferred_element_type=jnp.float32)
    dense_hidden = (jax.nn.silu(dense_gate) * dense_up).astype(jnp.bfloat16)
    running = jnp.einsum("rf,df->rd", dense_hidden, stacked[2], preferred_element_type=jnp.float32)
    for bit in reversed(range(shard_bits)):
        half = running.shape[0] // 2
        upper = own_index >> bit & 1 == 1
        keep = jnp.where(upper, running[half:], running[:half])
        give = jnp.where(upper, running[:half], running[half:])
        running = keep + partner_2(give.astype(jnp.bfloat16), "ep", bit).astype(give.dtype)
    local_expert = experts_by_exchange(
        settled,
        routes,
        route_weights,
        own_index,
        shards,
        expert_gate_weight,
        expert_up_weight,
        expert_down_weight,
    )
    ffn = dense_scale * running + local_expert
    return layer_norm(
        residual_scale * settled.astype(jnp.float32) + ffn, norm_gain[1], norm_bias[1]
    )


def solution(mesh):
    return jax.shard_map(
        local,
        mesh=mesh,
        in_specs=(
            P("ep", None),
            P("ep", None, None),
            P("ep", None, None),
            P("ep", None, None),
            P("ep"),
            P(),
            P(),
            P(),
            P(),
            P("ep", None),
            P(),
            P(),
            P(None, "ep"),
            P(None, "ep"),
            P("ep", None),
            P(),
            P(None, "ep"),
            P(None, "ep"),
            P("ep", None),
            P(),
            P(),
        ),
        out_specs=P("ep", None),
        check_vma=False,
    )
```

profile of v0, /device:TPU:0, one launch (start us, length us, event | category | flops | bytes accessed | tf_op | source)
XLA Modules:
  0.0 263.8 jit_solution(18136717045035868061)
XLA Ops:
  6.5 0.7 all-gather.2.cloned.1.call-update
  7.3 1.2 pad_maximum_fusion
  8.5 3.4 %collective-permute-start.4 = (bf16[3,2048,44]{1,2,0:T(8,128)(2,1)S(1)}, bf16[3,2048,44]{1,2,0:T(8,128)(2,1)S(1)}, u32[]{:S(2)}, u32[]{:S(2)}) collective-permute-start(bf16[3,2048,44]{1,2,0:T(8,128)(2,1)S(1)} %pad_maximum_fusion), channel_id=1, source_target_pairs={{0,16},{16,0},{1,17},{17,1},{2,18},{18,2},{3,19},{19,3},{4,20},{20... | collective-permute-start | bytes 1622024 | tf_op jit(solution)/shard_map/ppermute | solution.py:22
  11.9 3.9 %copy.50 = bf16[8,1024,128]{1,2,0:T(8,128)(2,1)} copy(bf16[8,1024,128]{2,1,0:T(8,128)(2,1)} %param.23) | data formatting | bytes 4194304 | tf_op args[2]
  16.0 2.6 copy.48
  18.6 4.6 %convolution_convert_fusion.2 = bf16[8,2048]{1,0:T(8,128)(2,1)S(1)} fusion(bf16[8,2048]{1,0:T(8,128)(2,1)S(1)} %copy-done.5, bf16[2048,2048]{1,0:T(8,128)(2,1)} %param.26), kind=kOutput, calls=%fused_computation.7 | convolution fusion | flops 67125248 | bytes 8454144 | tf_op jit(solution)/shard_map/dot_general | solution.py:164
  23.4 3.9 %copy.47 = bf16[8,1024,128]{1,2,0:T(8,128)(2,1)} copy(bf16[8,1024,128]{2,1,0:T(8,128)(2,1)} %param.22) | data formatting | bytes 4194304 | tf_op args[1]
  27.3 1.2 convolution_convert_fusion.4
  28.6 1.2 fusion.7
  30.0 1.3 gather_fusion
  31.7 2.1 fusion.46
  33.9 0.3 fusion.8
  34.2 0.4 maximum_select_fusion.2
  34.6 2.0 collective-permute-start.5
  36.6 0.7 fusion.6
  37.6 25.5 %collective-permute-done.5 = bf16[3,2048,88]{1,2,0:T(8,128)(2,1)} collective-permute-done((bf16[3,2048,88]{1,2,0:T(8,128)(2,1)S(1)}, bf16[3,2048,88]{1,2,0:T(8,128)(2,1)}, u32[]{:S(2)}, u32[]{:S(2)}) %collective-permute-start.5) | collective-permute-done | bytes 1081376 | tf_op jit(solution)/shard_map/ppermute | solution.py:22
  63.1 4.5 %maximum_select_fusion.1 = bf16[3,2048,176]{1,2,0:T(8,128)(2,1)} fusion(bf16[3,2048,88]{1,2,0:T(8,128)(2,1)S(1)} %maximum_select_fusion.2, bf16[3,2048,88]{1,2,0:T(8,128)(2,1)} %collective-permute-done.5, pred[]{:T(512)S(6)} %eq.71), kind=kLoop, calls=%fused_computation.8 | loop fusion | flops 9732096 | bytes 4325377 | tf_op jit(solution)/shard_map/jit(_where)/select_n | solution.py:159
  67.5 3.5 %collective-permute-start.6 = (bf16[3,2048,176]{1,2,0:T(8,128)(2,1)}, bf16[3,2048,176]{1,2,0:T(8,128)(2,1)}, u32[]{:S(2)}, u32[]{:S(2)}) collective-permute-start(bf16[3,2048,176]{1,2,0:T(8,128)(2,1)} %maximum_select_fusion.1), channel_id=1, source_target_pairs={{0,64},{64,0},{1,65},{65,1},{2,66},{66,2},{3,67},{67,3},{4,68},{68... | collective-permute-start | bytes 6488072 | tf_op jit(solution)/shard_map/ppermute | solution.py:22
  71.0 52.6 %all-gather.2.cloned.1.call-done = bf16[2048,2048]{1,0:T(8,128)(2,1)} async-done(((bf16[16,2048]{1,0:T(8,128)(2,1)}), bf16[2048,2048]{1,0:T(8,128)(2,1)}) %all-gather.2.cloned.1.call-update) | async-done | bytes 8388624 | tf_op jit(solution)/shard_map/all_gather | solution.py:177
  123.6 4.7 %fusion.47 = (f32[8]{0:T(128)S(1)}, f32[8,2048]{1,0:T(8,128)S(1)}) fusion(bf16[8,2048]{1,0:T(8,128)(2,1)S(1)} %convert_element_type.123, bf16[2048,2048]{1,0:T(8,128)(2,1)} %all-gather.2.cloned.1.call-done, bf16[8,2048]{1,0:T(8,128)(2,1)S(1)} %copy-done.5), kind=kOutput, calls=%fused_computation.107 | convolution fusion | flops 67174392 | bytes 8519712 | tf_op jit(solution)/shard_map/dot_general | solution.py:175
  128.7 1.2 collective-permute-done
  129.9 1.5 collective-permute-start.1
  131.5 2.8 %collective-permute-done.1 = bf16[16,2048]{1,0:T(8,128)(2,1)S(1)} collective-permute-done((bf16[16,2048]{1,0:T(8,128)(2,1)S(1)}, bf16[16,2048]{1,0:T(8,128)(2,1)S(1)}, u32[]{:S(2)}, u32[]{:S(2)}) %collective-permute-start.1) | collective-permute-done | bytes 65568 | tf_op jit(solution)/shard_map/ppermute | solution.py:22
  134.3 3.1 %collective-permute-start.2 = (bf16[32,2048]{1,0:T(8,128)(2,1)S(1)}, bf16[32,2048]{1,0:T(8,128)(2,1)S(1)}, u32[]{:S(2)}, u32[]{:S(2)}) collective-permute-start(bf16[32,2048]{1,0:T(8,128)(2,1)S(1)} %maximum_select_fusion.5), channel_id=1, source_target_pairs={{0,4},{4,0},{1,5},{5,1},{2,6},{6,2},{3,7},{7,3},{8,12},{12,8},{9,1... | collective-permute-start | bytes 393224 | tf_op jit(solution)/shard_map/ppermute | solution.py:22
  137.3 0.7 constant_dynamic-slice_fusion.1
  138.2 2.6 collective-permute-done.2
  140.9 1.1 collective-permute-start.3
  141.9 6.2 %maximum_select_fusion = bf16[3,2048,352]{1,2,0:T(8,128)(2,1)} fusion(bf16[3,2048,176]{1,2,0:T(8,128)(2,1)} %maximum_select_fusion.1, bf16[3,2048,176]{1,2,0:T(8,128)(2,1)} %collective-permute-done.6, pred[]{:T(512)S(6)} %eq.70), kind=kLoop, calls=%fused_computation.1 | loop fusion | flops 19464192 | bytes 8650753 | tf_op jit(solution)/shard_map/jit(_where)/select_n | solution.py:159
  148.1 0.2 convolution_convert_fusion.1
  148.4 2.4 broadcast_in_dim.21
  150.8 12.5 %all-to-all-start = ((bf16[128,3,2048]{2,1,0:T(4,128)(2,1)}), bf16[128,3,2048]{2,1,0:T(4,128)(2,1)}, u32[]{:S(2)}, u32[]{:S(2)}) async-start(bf16[128,3,2048]{2,1,0:T(4,128)(2,1)} %bitcast.66), calls=%async_computation | async-start | bytes 4194304 | tf_op jit(solution)/shard_map/all_to_all | solution.py:116
  163.3 0.7 copy-done.11
  164.0 2.6 fusion.1
  166.6 3.5 %fusion = f32[128,2048]{1,0:T(8,128)S(1)} fusion(bf16[3,2048,352]{1,2,0:T(8,128)(2,1)} %maximum_select_fusion, f32[128,352]{0,1:T(8,128)} %fusion.1, bf16[64,2048]{1,0:T(8,128)(2,1)S(1)} %maximum_select_fusion.4, bf16[64,2048]{1,0:T(8,128)(2,1)} %copy-done.11, pred[]{:T(512)S(6)} %eq.69), kind=kOutput, calls=%fused_computation.10 | convolution fusion | flops 371728384 | bytes 4636673 | tf_op jit(solution)/shard_map/rf,df->rd/dot_general | solution.py:195
  170.2 0.8 collective-permute-start.7
  171.0 0.7 constant_dynamic-slice_fusion
  171.7 20.2 %collective-permute-done.7 = bf16[64,2048]{1,0:T(8,128)(2,1)S(1)} collective-permute-done((bf16[64,2048]{1,0:T(8,128)(2,1)S(1)}, bf16[64,2048]{1,0:T(8,128)(2,1)S(1)}, u32[]{:S(2)}, u32[]{:S(2)}) %collective-permute-start.7) | collective-permute-done | bytes 262176 | tf_op jit(solution)/shard_map/ppermute | solution.py:22
  192.0 3.0 %collective-permute-start.8 = (bf16[32,2048]{1,0:T(8,128)(2,1)S(1)}, bf16[32,2048]{1,0:T(8,128)(2,1)S(1)}, u32[]{:S(2)}, u32[]{:S(2)}) collective-permute-start(bf16[32,2048]{1,0:T(8,128)(2,1)S(1)} %select_convert_fusion.1), channel_id=1, source_target_pairs={{0,4},{4,0},{1,5},{5,1},{2,6},{6,2},{3,7},{7,3},{8,12},{12,8},{9,1... | collective-permute-start | bytes 393224 | tf_op jit(solution)/shard_map/ppermute | solution.py:22
  195.1 5.0 %reshape.158 = bf16[384,2048]{1,0:T(8,128)(2,1)} reshape(bf16[128,3,2048]{2,1,0:T(4,128)(2,1)} %all-to-all-done) | data formatting | bytes 3145728 | tf_op jit(solution)/shard_map/reshape | solution.py:117
  200.1 3.1 %fusion.49 = f32[384,448]{0,1:T(8,128)S(1)} fusion(bf16[384,2048]{1,0:T(8,128)(2,1)} %reshape.158, bf16[2048,448]{0,1:T(8,128)(2,1)} %param.37), kind=kOutput, calls=%fused_computation.109 | convolution fusion | flops 704643072 | bytes 4096000 | tf_op jit(solution)/shard_map/dot_general | solution.py:87
  203.2 5.2 %convolution_convert_fusion = bf16[384,2048]{1,0:T(8,128)(2,1)} fusion(bf16[448,2048]{1,0:T(8,128)(2,1)S(1)} %copy-done, bf16[384,2048]{1,0:T(8,128)(2,1)} %reshape.158, bf16[2048,448]{0,1:T(8,128)(2,1)} %param.38, f32[384,448]{0,1:T(8,128)S(1)} %fusion.49), kind=kOutput, calls=%fused_computation.3 | convolution fusion | flops 1411104768 | bytes 7503872 | tf_op jit(solution)/shard_map/dot_general | solution.py:90
  208.5 5.1 %reshape.159 = bf16[128,3,2048]{2,1,0:T(4,128)(2,1)} reshape(bf16[384,2048]{1,0:T(8,128)(2,1)} %convolution_convert_fusion) | data formatting | bytes 3145728 | tf_op jit(solution)/shard_map/reshape | solution.py:119
  213.6 8.7 %all-to-all-start.1 = ((bf16[128,3,2048]{2,1,0:T(4,128)(2,1)}), bf16[128,3,2048]{2,1,0:T(4,128)(2,1)}, u32[]{:S(2)}, u32[]{:S(2)}) async-start(bf16[128,3,2048]{2,1,0:T(4,128)(2,1)} %reshape.159), calls=%async_computation.1 | async-start | bytes 4194304 | tf_op jit(solution)/shard_map/all_to_all | solution.py:120
  222.5 1.0 collective-permute-start.9
  223.5 23.5 %collective-permute-done.9 = bf16[16,2048]{1,0:T(8,128)(2,1)S(1)} collective-permute-done((bf16[16,2048]{1,0:T(8,128)(2,1)S(1)}, bf16[16,2048]{1,0:T(8,128)(2,1)S(1)}, u32[]{:S(2)}, u32[]{:S(2)}) %collective-permute-start.9) | collective-permute-done | bytes 65568 | tf_op jit(solution)/shard_map/ppermute | solution.py:22
  247.1 5.8 %all-to-all-done.1 = bf16[128,3,2048]{2,1,0:T(4,128)(2,1)} async-done(((bf16[128,3,2048]{2,1,0:T(4,128)(2,1)}), bf16[128,3,2048]{2,1,0:T(4,128)(2,1)}, u32[]{:S(2)}, u32[]{:S(2)}) %all-to-all-start.1) | async-done | bytes 1572896 | tf_op jit(solution)/shard_map/all_to_all | solution.py:120
  252.9 2.7 %convert_reduce_fusion = bf16[8,3,2048]{2,1,0:T(4,128)(2,1)S(1)} fusion(bf16[128,3,2048]{2,1,0:T(4,128)(2,1)} %all-to-all-done.1), kind=kLoop, calls=%fused_computation.2 | loop fusion | flops 1523712 | bytes 1671168 | tf_op jit(solution)/shard_map/reduce_sum | solution.py:121
  256.2 0.7 add_convert_fusion
  (77 shorter events, 3.0 us)
Async XLA Ops:
  6.5 196.7 %copy-start = (bf16[448,2048]{1,0:T(8,128)(2,1)S(1)}, bf16[448,2048]{1,0:T(8,128)(2,1)}, u32[]{:S(2)}) copy-start(bf16[448,2048]{1,0:T(8,128)(2,1)} %param.39) | copy-start | bytes 5505028
  6.5 117.1 %all-gather.2.cloned.1.call-start = ((), (), s32[]{:S(2)}) async-start(), calls=%async_computation.2 | async-start | bytes 8454144 | tf_op jit(solution)/shard_map/all_gather | solution.py:177
  8.5 7.3 %copy-start.5 = (bf16[8,2048]{1,0:T(8,128)(2,1)S(1)}, bf16[8,2048]{1,0:T(8,128)(2,1)}, u32[]{:S(2)}) copy-start(bf16[8,2048]{1,0:T(8,128)(2,1)} %param.21) | copy-start | bytes 98308
  8.5 7.3 %copy-start.12 = (bf16[2048,2]{0,1:T(2,128)(2,1)S(1)}, bf16[2048,2]{0,1:T(2,128)(2,1)}, u32[]{:S(2)}) copy-start(bf16[2048,2]{0,1:T(2,128)(2,1)} %param.29) | copy-start | bytes 24580
  8.5 7.5 %copy-start.6 = (f32[8,1024,2]{1,2,0:T(2,128)S(1)}, f32[8,1024,2]{1,2,0:T(2,128)}, u32[]{:S(2)}) copy-start(f32[8,1024,2]{1,2,0:T(2,128)} %param.24) | copy-start | bytes 196612
  8.5 25.7 %collective-permute-start.4 = (bf16[3,2048,44]{1,2,0:T(8,128)(2,1)S(1)}, bf16[3,2048,44]{1,2,0:T(8,128)(2,1)S(1)}, u32[]{:S(2)}, u32[]{:S(2)}) collective-permute-start(bf16[3,2048,44]{1,2,0:T(8,128)(2,1)S(1)} %pad_maximum_fusion), channel_id=1, source_target_pairs={{0,16},{16,0},{1,17},{17,1},{2,18},{18,2},{3,19},{19,3},{4,20},{20... | collective-permute-start | bytes 1622024 | tf_op jit(solution)/shard_map/ppermute | solution.py:22
  23.3 6.6 %copy-start.10 = (s32[8]{0:T(128)S(1)}, s32[8]{0:T(128)}, u32[]{:S(2)}) copy-start(s32[8]{0:T(128)} %param.25) | copy-start | bytes 100
  31.6 2.6 copy-start.2
  31.7 2.6 copy-start.3
  31.7 2.6 copy-start.4
  33.8 2.8 %copy-start.1 = (bf16[8,1024,128]{1,2,0:T(8,128)(2,1)S(1)}, bf16[8,1024,128]{1,2,0:T(8,128)(2,1)}, u32[]{:S(2)}) copy-start(bf16[8,1024,128]{1,2,0:T(8,128)(2,1)} %copy.50) | copy-start | bytes 6291460
  34.6 28.4 %collective-permute-start.5 = (bf16[3,2048,88]{1,2,0:T(8,128)(2,1)S(1)}, bf16[3,2048,88]{1,2,0:T(8,128)(2,1)}, u32[]{:S(2)}, u32[]{:S(2)}) collective-permute-start(bf16[3,2048,88]{1,2,0:T(8,128)(2,1)S(1)} %maximum_select_fusion.2), channel_id=1, source_target_pairs={{0,32},{32,0},{1,33},{33,1},{2,34},{34,2},{3,35},{35,3},{4,36},{36... | collective-permute-start | bytes 3244040 | tf_op jit(solution)/shard_map/ppermute | solution.py:22
  36.6 0.9 copy-start.7
  36.6 0.9 copy-start.8
  67.5 74.4 %collective-permute-start.6 = (bf16[3,2048,176]{1,2,0:T(8,128)(2,1)}, bf16[3,2048,176]{1,2,0:T(8,128)(2,1)}, u32[]{:S(2)}, u32[]{:S(2)}) collective-permute-start(bf16[3,2048,176]{1,2,0:T(8,128)(2,1)} %maximum_select_fusion.1), channel_id=1, source_target_pairs={{0,64},{64,0},{1,65},{65,1},{2,66},{66,2},{3,67},{67,3},{4,68},{68... | collective-permute-start | bytes 6488072 | tf_op jit(solution)/shard_map/ppermute | solution.py:22
  128.6 1.3 collective-permute-start
  129.9 4.3 %collective-permute-start.1 = (bf16[16,2048]{1,0:T(8,128)(2,1)S(1)}, bf16[16,2048]{1,0:T(8,128)(2,1)S(1)}, u32[]{:S(2)}, u32[]{:S(2)}) collective-permute-start(bf16[16,2048]{1,0:T(8,128)(2,1)S(1)} %maximum_select_fusion.9), channel_id=1, source_target_pairs={{0,2},{2,0},{1,3},{3,1},{4,6},{6,4},{5,7},{7,5},{8,10},{10,8},{9,1... | collective-permute-start | bytes 196616 | tf_op jit(solution)/shard_map/ppermute | solution.py:22
  134.3 6.6 %collective-permute-start.2 = (bf16[32,2048]{1,0:T(8,128)(2,1)S(1)}, bf16[32,2048]{1,0:T(8,128)(2,1)S(1)}, u32[]{:S(2)}, u32[]{:S(2)}) collective-permute-start(bf16[32,2048]{1,0:T(8,128)(2,1)S(1)} %maximum_select_fusion.5), channel_id=1, source_target_pairs={{0,4},{4,0},{1,5},{5,1},{2,6},{6,2},{3,7},{7,3},{8,12},{12,8},{9,1... | collective-permute-start | bytes 393224 | tf_op jit(solution)/shard_map/ppermute | solution.py:22
  140.9 22.4 %collective-permute-start.3 = (bf16[64,2048]{1,0:T(8,128)(2,1)S(1)}, bf16[64,2048]{1,0:T(8,128)(2,1)S(1)}, u32[]{:S(2)}, u32[]{:S(2)}) collective-permute-start(bf16[64,2048]{1,0:T(8,128)(2,1)S(1)} %maximum_select_fusion.4), channel_id=1, source_target_pairs={{0,8},{8,0},{1,9},{9,1},{2,10},{10,2},{3,11},{11,3},{4,12},{12,4},... | collective-permute-start | bytes 786440 | tf_op jit(solution)/shard_map/ppermute | solution.py:22
  150.8 44.3 %all-to-all-start = ((bf16[128,3,2048]{2,1,0:T(4,128)(2,1)}), bf16[128,3,2048]{2,1,0:T(4,128)(2,1)}, u32[]{:S(2)}, u32[]{:S(2)}) async-start(bf16[128,3,2048]{2,1,0:T(4,128)(2,1)} %bitcast.66), calls=%async_computation | async-start | bytes 4194304 | tf_op jit(solution)/shard_map/all_to_all | solution.py:116
  163.3 0.7 copy-start.11
  170.2 21.8 %collective-permute-start.7 = (bf16[64,2048]{1,0:T(8,128)(2,1)S(1)}, bf16[64,2048]{1,0:T(8,128)(2,1)S(1)}, u32[]{:S(2)}, u32[]{:S(2)}) collective-permute-start(bf16[64,2048]{1,0:T(8,128)(2,1)S(1)} %select_convert_fusion), channel_id=1, source_target_pairs={{0,8},{8,0},{1,9},{9,1},{2,10},{10,2},{3,11},{11,3},{4,12},{12,4},... | collective-permute-start | bytes 786440 | tf_op jit(solution)/shard_map/ppermute | solution.py:22
  192.0 30.3 %collective-permute-start.8 = (bf16[32,2048]{1,0:T(8,128)(2,1)S(1)}, bf16[32,2048]{1,0:T(8,128)(2,1)S(1)}, u32[]{:S(2)}, u32[]{:S(2)}) collective-permute-start(bf16[32,2048]{1,0:T(8,128)(2,1)S(1)} %select_convert_fusion.1), channel_id=1, source_target_pairs={{0,4},{4,0},{1,5},{5,1},{2,6},{6,2},{3,7},{7,3},{8,12},{12,8},{9,1... | collective-permute-start | bytes 393224 | tf_op jit(solution)/shard_map/ppermute | solution.py:22
  213.6 39.2 %all-to-all-start.1 = ((bf16[128,3,2048]{2,1,0:T(4,128)(2,1)}), bf16[128,3,2048]{2,1,0:T(4,128)(2,1)}, u32[]{:S(2)}, u32[]{:S(2)}) async-start(bf16[128,3,2048]{2,1,0:T(4,128)(2,1)} %reshape.159), calls=%async_computation.1 | async-start | bytes 4194304 | tf_op jit(solution)/shard_map/all_to_all | solution.py:120
  222.4 33.4 %copy-start.9 = (f32[2048]{0:T(1024)S(1)}, f32[2048]{0:T(1024)}, u32[]{:S(2)}) copy-start(f32[2048]{0:T(1024)} %param.36) | copy-start | bytes 24580
  222.5 24.5 %collective-permute-start.9 = (bf16[16,2048]{1,0:T(8,128)(2,1)S(1)}, bf16[16,2048]{1,0:T(8,128)(2,1)S(1)}, u32[]{:S(2)}, u32[]{:S(2)}) collective-permute-start(bf16[16,2048]{1,0:T(8,128)(2,1)S(1)} %select_convert_fusion.2), channel_id=1, source_target_pairs={{0,2},{2,0},{1,3},{3,1},{4,6},{6,4},{5,7},{7,5},{8,10},{10,8},{9,1... | collective-permute-start | bytes 196616 | tf_op jit(solution)/shard_map/ppermute | solution.py:22
  247.0 8.8 %collective-permute-start.10 = (bf16[8,2048]{1,0:T(8,128)(2,1)S(1)}, bf16[8,2048]{1,0:T(8,128)(2,1)S(1)}, u32[]{:S(2)}, u32[]{:S(2)}) collective-permute-start(bf16[8,2048]{1,0:T(8,128)(2,1)S(1)} %select_convert_fusion.3), channel_id=1, source_target_pairs={{0,1},{1,0},{2,3},{3,2},{4,5},{5,4},{6,7},{7,6},{8,9},{9,8},{10,11... | collective-permute-start | bytes 98312 | tf_op jit(solution)/shard_map/ppermute | solution.py:22
Sparse Core Ops, SparseCore 0:
  10.3 113.2 all-gather.1
where the time goes:
time: 265 us; the launch traced here: 264 us
  waiting for transfers between devices  135 us (51%)
  starting transfers between devices  40.8 us (15%)
  matrix products  29.7 us (11%)
  local copies, waits for them, and re-layouts  27.2 us (10%)
  other arithmetic  17.5 us (7%)
  between operations  13.8 us (5%)
    ppermute x11, waiting for transfers between devices, partner_2(): return lax.ppermute(block, axis, route)  75.8 us
    all_gather x1, waiting for transfers between devices, local(): lax.all_gather(out_weight, 'ep', axis=0, tiled=True)  52.6 us
    ppermute x11, starting transfers between devices, partner_2(): return lax.ppermute(block, axis, route)  19.5 us
    all_to_all x1, starting transfers between devices, experts_by_exchange(): lax.all_to_all(outgoing, 'ep', split_axis=0, concat_axis=0, tiled=True)  12.5 us
    unnamed x30, local copies, waits for them, and re-layouts  11.2 us
    select_n x3, other arithmetic, local(): jnp.where(upper, jnp.concatenate([partner, stacked], axis=2), jnp.concate...  11 us
    all_to_all x1, starting transfers between devices, experts_by_exchange(): lax.all_to_all(answered, 'ep', split_axis=0, concat_axis=0, tiled=True)  8.75 us
    all_to_all x1, waiting for transfers between devices, experts_by_exchange(): lax.all_to_all(answered, 'ep', split_axis=0, concat_axis=0, tiled=True)  5.76 us
  transfers between devices with their start and end apart: 14, of which 8 were waited for; matrix products, arithmetic and copies ran while one was open for 27% of the time, Pallas kernels for 0%

commit v1 on v0

v1 whole, which is shorter than its diff:
```python
import jax
import jax.numpy as jnp
from jax import lax
from jax.sharding import PartitionSpec as P

EXPERTS = 8
TOP = 2
CAP = 3


residual_scale = 1.4142135
norm_eps = 1e-05


CHIPS = 64
SLOTS = 5
GROUP_Z = 4

CORE_GROUPS = [[2 * chip + core for chip in range(64)] for core in range(2)]
ROW_GROUPS = [[8 * ring + place for place in range(8)] for ring in range(16)]
WEIGHT_GROUPS = [[8 * ring + place for ring in range(16)] for place in range(8)]


def shift_z(block, step):
    return lax.ppermute(block, "ep", [(i, (i + 32 * step) % 128) for i in range(128)])


def swap_core(block):
    return lax.ppermute(block, "ep", [(i, i ^ 1) for i in range(128)])


def exchange(block, groups):
    return lax.all_to_all(
        block, "ep", split_axis=0, concat_axis=0, axis_index_groups=groups, tiled=True
    )


def layer_norm(values, gain_row, shift_row):
    centre = jnp.mean(values, axis=-1, keepdims=True)
    centred = values - centre
    spread = jnp.mean(centred * centred, axis=-1, keepdims=True)
    return (centred * lax.rsqrt(spread + norm_eps) * gain_row + shift_row).astype(jnp.bfloat16)


def attend(
    queries, cached_keys, cached_values, gate_sums, length_row, fresh_key, fresh_value, fresh_gate
):
    amount = queries.shape[0]
    cache_len = cached_keys.shape[1]
    kv_count = fresh_gate.shape[1]
    head_dim = fresh_key.shape[1] // kv_count
    grouped = queries.shape[1] // (kv_count * head_dim)
    query_grid_four = queries.reshape(amount, kv_count, grouped, head_dim)
    key_four = cached_keys.reshape(amount, cache_len, kv_count, head_dim)
    value_four = cached_values.reshape(amount, cache_len, kv_count, head_dim)
    self_key_row = fresh_key.reshape(amount, kv_count, head_dim)
    own_value = fresh_value.astype(jnp.float32).reshape(amount, kv_count, head_dim)
    ratio_value = head_dim ** (-0.5)
    latest = jnp.take_along_axis(gate_sums, (length_row - 1)[:, None, None], axis=1)
    offsets = jnp.transpose(latest - gate_sums + fresh_gate[:, None, :], (0, 2, 1))
    past = jnp.einsum(
        "bkgd,blkd->bkgl", query_grid_four, key_four, preferred_element_type=jnp.float32
    )
    past = past * ratio_value + offsets[:, :, None, :]
    live = jnp.arange(cache_len, dtype=jnp.int32)[None, :] < length_row[:, None]
    past = jnp.where(live[:, None, None, :], past, -jnp.inf)
    self_part = (
        jnp.einsum(
            "rifs,ris->rif", query_grid_four, self_key_row, preferred_element_type=jnp.float32
        )
        * ratio_value
    )
    highest = jnp.maximum(jnp.max(past, axis=-1), self_part)
    past_exp = jnp.exp(past - highest[..., None])
    own_exp = jnp.exp(self_part - highest)
    denominator = jnp.sum(past_exp, axis=-1) + own_exp
    past_weight = (past_exp / denominator[..., None]).astype(jnp.bfloat16)
    own_weight = (own_exp / denominator).astype(jnp.bfloat16)
    mixed = jnp.einsum(
        "bkgl,blkd->bkgd", past_weight, value_four, preferred_element_type=jnp.float32
    )
    mixed = mixed + own_weight.astype(jnp.float32)[..., None] * own_value[:, :, None, :]
    return mixed.reshape(amount, queries.shape[1]).astype(jnp.bfloat16)


def slot_tables(chosen, shares):
    expert_ids = jnp.arange(EXPERTS, dtype=jnp.int32)
    picked = (chosen[..., None] == expert_ids).astype(jnp.int32)
    hits = jnp.sum(picked, axis=1)
    portion = jnp.sum(picked.astype(jnp.float32) * shares[..., None], axis=1)
    ranks = jnp.cumsum(hits, axis=0) - hits
    slot_ids = jnp.arange(CAP, dtype=jnp.int32)
    matched = (hits[..., None] * (ranks[..., None] == slot_ids).astype(jnp.int32)).astype(
        jnp.float32
    )
    return (matched, portion)


def gather_dense(gate_cols, up_cols, down_rows):
    short = ((0, 4), (0, 0))
    own = jnp.concatenate(
        [
            jnp.pad(jnp.transpose(gate_cols), short),
            jnp.pad(jnp.transpose(up_cols), short),
            jnp.pad(down_rows, short),
        ],
        axis=0,
    )
    half = own.shape[0] // 2
    before = shift_z(own, 1)
    after = shift_z(own, -1)
    far_low = shift_z(before[:half], 1)
    far_high = shift_z(after[half:], -1)
    mine = jnp.concatenate([own, before, after, far_low, far_high], axis=0)
    both = jnp.concatenate([mine, swap_core(mine)], axis=0)
    parts = both.reshape(8, 3, 48, 2048)
    return [parts[:, i].reshape(384, 2048) for i in range(3)]


def local(
    tokens,
    cache_keys,
    cache_values,
    cum_gates,
    lengths,
    query_weight,
    key_weight,
    value_weight,
    forget_weight,
    out_weight,
    norm_gain,
    norm_bias,
    dense_gate_weight,
    dense_up_weight,
    dense_down_weight,
    dense_scale,
    expert_gate_weight,
    expert_up_weight,
    expert_down_weight,
    routes,
    route_weights,
):
    own_index = lax.axis_index("ep")
    rows, width = tokens.shape
    out_rows = exchange(jnp.tile(out_weight, (16, 1)), WEIGHT_GROUPS)
    dense_gate_rows, dense_up_rows, dense_down_all = gather_dense(
        dense_gate_weight, dense_up_weight, dense_down_weight
    )
    query = jnp.dot(tokens, query_weight, preferred_element_type=jnp.float32).astype(jnp.bfloat16)
    new_key = jnp.dot(tokens, key_weight, preferred_element_type=jnp.float32).astype(jnp.bfloat16)
    new_value = jnp.dot(tokens, value_weight, preferred_element_type=jnp.float32).astype(
        jnp.bfloat16
    )
    new_gate = jax.nn.log_sigmoid(
        jnp.dot(tokens, forget_weight, preferred_element_type=jnp.float32)
    )
    attended = attend(
        query, cache_keys, cache_values, cum_gates, lengths, new_key, new_value, new_gate
    )
    slices = jnp.transpose(attended.reshape(rows, 16, 8, 16), (2, 0, 1, 3)).reshape(64, 256)
    slices = exchange(slices, ROW_GROUPS)
    partial = jnp.dot(slices, out_rows, preferred_element_type=jnp.float32).astype(jnp.bfloat16)
    partial = exchange(partial, ROW_GROUPS)
    projected = jnp.sum(partial.reshape(8, rows, width).astype(jnp.float32), axis=0)
    settled = layer_norm(
        residual_scale * tokens.astype(jnp.float32) + projected, norm_gain[0], norm_bias[0]
    )
    own_routes = lax.dynamic_slice_in_dim(routes, own_index * rows, rows, 0)
    own_shares = lax.dynamic_slice_in_dim(route_weights, own_index * rows, rows, 0)
    matched, portion = slot_tables(own_routes, own_shares)
    expert_ids = jnp.arange(EXPERTS, dtype=jnp.int32)
    pair_row = 2 * (expert_ids // 2)[:, None] + jnp.arange(2, dtype=jnp.int32)[None, :]
    dense_pick = (pair_row[..., None] == jnp.arange(rows, dtype=jnp.int32)).astype(jnp.bfloat16)
    picks = jnp.concatenate(
        [jnp.transpose(matched, (1, 2, 0)).astype(jnp.bfloat16), dense_pick], axis=1
    )
    messages = jnp.einsum(
        "ekr,rsc->eskc",
        picks,
        settled.reshape(rows, 8, 256),
        preferred_element_type=jnp.float32,
    ).astype(jnp.bfloat16)
    outgoing = jnp.repeat(messages.reshape(EXPERTS, 1, 8, SLOTS * 256), 8, axis=1)
    received = exchange(outgoing.reshape(CHIPS * 8, SLOTS * 256), CORE_GROUPS)
    arrived = jnp.transpose(received.reshape(CHIPS, 8, SLOTS, 256), (2, 0, 1, 3)).reshape(
        SLOTS, CHIPS, width
    )
    expert_rows = arrived[:CAP].reshape(CAP * CHIPS, width)
    dense_rows = arrived[CAP:].reshape(2 * CHIPS, width)
    other_rows = swap_core(expert_rows)
    contract = (((1,), (1,)), ((), ()))
    gate_val = lax.dot_general(
        dense_rows, dense_gate_rows, contract, preferred_element_type=jnp.float32
    )
    up_val = lax.dot_general(
        dense_rows, dense_up_rows, contract, preferred_element_type=jnp.float32
    )
    dense_hidden = (jax.nn.silu(gate_val) * up_val).astype(jnp.bfloat16)
    dense_part = jnp.dot(dense_hidden, dense_down_all, preferred_element_type=jnp.float32)
    both_rows = jnp.concatenate([expert_rows, other_rows], axis=0)
    gate_val = jnp.dot(both_rows, expert_gate_weight, preferred_element_type=jnp.float32)
    up_val = jnp.dot(both_rows, expert_up_weight, preferred_element_type=jnp.float32)
    hidden = (jax.nn.silu(gate_val) * up_val).astype(jnp.bfloat16)
    result = jnp.dot(hidden, expert_down_weight, preferred_element_type=jnp.float32)
    half = CAP * CHIPS
    result_mine = result[:half] + swap_core(result[half:].astype(jnp.bfloat16)).astype(jnp.float32)
    answers = jnp.concatenate([result_mine, dense_part], axis=0).astype(jnp.bfloat16)
    answers = jnp.transpose(answers.reshape(SLOTS, CHIPS, 8, 256), (1, 2, 0, 3))
    returned = exchange(answers.reshape(CHIPS * 8, SLOTS * 256), CORE_GROUPS)
    returned = returned.reshape(CHIPS, 8, SLOTS, 256).astype(jnp.float32)
    expert_sum = jnp.sum(returned[:, :, :CAP].reshape(EXPERTS, 8, 8, CAP, 256), axis=1)
    dense_sum = jnp.sum(returned[:, :, CAP:].reshape(GROUP_Z, 16, 8, 2, 256), axis=1)
    dense_out = jnp.transpose(dense_sum, (0, 2, 1, 3)).reshape(rows, width)
    expert_out = jnp.einsum("rek,eskc->rsc", matched * portion[..., None], expert_sum).reshape(
        rows, width
    )
    ffn = dense_scale * dense_out + expert_out
    return layer_norm(
        residual_scale * settled.astype(jnp.float32) + ffn, norm_gain[1], norm_bias[1]
    )


def solution(mesh):
    return jax.shard_map(
        local,
        mesh=mesh,
        in_specs=(
            P("ep", None),
            P("ep", None, None),
            P("ep", None, None),
            P("ep", None, None),
            P("ep"),
            P(),
            P(),
            P(),
            P(),
            P("ep", None),
            P(),
            P(),
            P(None, "ep"),
            P(None, "ep"),
            P("ep", None),
            P(),
            P(None, "ep"),
            P(None, "ep"),
            P("ep", None),
            P(),
            P(),
        ),
        out_specs=P("ep", None),
        check_vma=False,
    )
```

time: 265 us -> 176 us (0.66)
  waiting for transfers between devices: 135 us -> 35.2 us
  blocking collectives: 0 us -> 26.9 us
  local copies, waits for them, and re-layouts: 27.2 us -> 50.1 us
  between operations: 13.8 us -> 0.42 us
  starting transfers between devices: 40.8 us -> 28.3 us
  other arithmetic: 17.5 us -> 9.12 us
  matrix products: 29.7 us -> 24.2 us
    ppermute x11 -> x7, waiting for transfers between devices: 75.8 us -> 8.86 us  [the longest x4 8.85 us: shift_z(): lax.ppermute(block, 'ep', [(i, (i + 32 * step) % 128) for i in range(128)])]
    all_gather x1 -> x0, waiting for transfers between devices: 52.6 us -> none  [local(): lax.all_gather(out_weight, 'ep', axis=0, tiled=True)]
    all_to_all x0 -> x1, blocking collectives: none -> 26.9 us  [exchange(): lax.all_to_all(block, 'ep', split_axis=0, concat_axis=0, axis_index_group...]
    all_to_all x2 -> x4, waiting for transfers between devices: 5.76 us -> 26.3 us  [exchange(): lax.all_to_all(block, 'ep', split_axis=0, concat_axis=0, axis_index_group...]
    unnamed x30 -> x53, local copies, waits for them, and re-layouts: 11.2 us -> 23 us
    select_n x6 -> x0, other arithmetic: 11.1 us -> none  [the longest x3 11 us: local(): jnp.where(upper, jnp.concatenate([partner, stacked], axis=2), jnp.concate...]
    ppermute x11 -> x7, starting transfers between devices: 19.5 us -> 8.72 us  [the longest x4 7.46 us: shift_z(): lax.ppermute(block, 'ep', [(i, (i + 32 * step) % 128) for i in range(128)])]
    reshape x2 -> x0, local copies, waits for them, and re-layouts: 10.2 us -> none  [the longest x1 5.15 us: experts_by_exchange(): answered = result.reshape(received.shape)]
  transfers between devices with their start and end apart: 14 -> 11, of which waited for: 8 -> 4; matrix products, arithmetic and copies ran while one was open for 27% -> 34% of each run, Pallas kernels for 0% -> 0%
where the time goes in v1:
time: 176 us; the launch traced here: 174 us
  local copies, waits for them, and re-layouts  50.1 us (28%)
  waiting for transfers between devices  35.2 us (20%)
  starting transfers between devices  28.3 us (16%)
  blocking collectives  26.9 us (15%)
  matrix products  24.2 us (14%)
  other arithmetic  9.12 us (5%)
    all_to_all x1, blocking collectives, exchange(): lax.all_to_all(block, 'ep', split_axis=0, concat_axis=0, axis_index_group...  26.9 us
    all_to_all x4, waiting for transfers between devices, exchange(): lax.all_to_all(block, 'ep', split_axis=0, concat_axis=0, axis_index_group...  26.3 us
    unnamed x53, local copies, waits for them, and re-layouts  23 us
    all_to_all x4, starting transfers between devices, exchange(): lax.all_to_all(block, 'ep', split_axis=0, concat_axis=0, axis_index_group...  19.6 us
    ppermute x4, waiting for transfers between devices, shift_z(): lax.ppermute(block, 'ep', [(i, (i + 32 * step) % 128) for i in range(128)])  8.85 us
    ppermute x4, starting transfers between devices, shift_z(): lax.ppermute(block, 'ep', [(i, (i + 32 * step) % 128) for i in range(128)])  7.46 us
    dot_general x1, matrix products, local(): jnp.dot(hidden, expert_down_weight, preferred_element_type=jnp.float32)  5.39 us
    dot_general x1, matrix products, local(): jnp.dot(tokens, query_weight, preferred_element_type=jnp.float32)  4.57 us
  transfers between devices with their start and end apart: 11, of which 4 were waited for; matrix products, arithmetic and copies ran while one was open for 34% of the time, Pallas kernels for 0%

profile of v1, /device:TPU:0, one launch (start us, length us, event | category | flops | bytes accessed | tf_op | source)
XLA Modules:
  0.0 174.2 jit_solution(12921266558596577189)
XLA Ops:
  0.0 1.9 %constant_dynamic-update-slice_fusion.8 = (bf16[576,2048]{1,0:T(8,128)(2,1)}, bf16[1152,2048]{1,0:T(8,128)(2,1)}, bf16[48,2048]{1,0:T(8,128)(2,1)S(1)}) fusion(bf16[44,2048]{1,0:T(8,128)(2,1)} %bitcast.137), kind=kLoop, calls=%fused_computation.58 | loop fusion | bytes 770048
  1.9 1.7 %constant_dynamic-update-slice_fusion.7 = (bf16[576,2048]{1,0:T(8,128)(2,1)}, bf16[1152,2048]{1,0:T(8,128)(2,1)}, bf16[48,2048]{1,0:T(8,128)(2,1)S(1)}) fusion(bf16[576,2048]{1,0:T(8,128)(2,1)} %get-tuple-element.22, bf16[44,2048]{1,0:T(8,128)(2,1)} %bitcast.138, bf16[1152,2048]{1,0:T(8,128)(2,1)} %get-tuple-element.23), kind=kLoop, calls=%fused_computation.57 | loop fusion | bytes 786432
  3.7 1.7 constant_dynamic-update-slice_fusion.6
  5.4 0.9 pad_maximum_fusion.1
  6.3 2.0 %collective-permute-start.2 = (bf16[144,2048]{1,0:T(8,128)(2,1)}, bf16[144,2048]{1,0:T(8,128)(2,1)}, u32[]{:S(2)}, u32[]{:S(2)}) collective-permute-start(bf16[144,2048]{1,0:T(8,128)(2,1)} %pad_maximum_fusion.1), channel_id=1, source_target_pairs={{0,32},{1,33},{2,34},{3,35},{4,36},{5,37},{6,38},{7,39},{8,40},{9,... | collective-permute-start | bytes 1769480 | tf_op jit(solution)/shard_map/ppermute | solution.py:25
  8.3 2.1 %collective-permute-start.3 = (bf16[144,2048]{1,0:T(8,128)(2,1)}, bf16[144,2048]{1,0:T(8,128)(2,1)S(1)}, u32[]{:S(2)}, u32[]{:S(2)}) collective-permute-start(bf16[144,2048]{1,0:T(8,128)(2,1)} %pad_maximum_fusion.1), channel_id=1, source_target_pairs={{0,96},{1,97},{2,98},{3,99},{4,100},{5,101},{6,102},{7,103},{8,104... | collective-permute-start | bytes 1769480 | tf_op jit(solution)/shard_map/ppermute | solution.py:25
  10.5 4.0 %copy.85 = bf16[8,1024,128]{1,2,0:T(8,128)(2,1)} copy(bf16[8,1024,128]{2,1,0:T(8,128)(2,1)} %param.23) | data formatting | bytes 4194304 | tf_op args[2]
  14.8 2.7 %copy.83 = f32[8,1024,2]{2,1,0:T(8,128)} copy(f32[8,1024,2]{1,2,0:T(2,128)S(1)} %copy-done.6) | data formatting | bytes 131072 | tf_op args[3]
  17.5 4.6 %convolution_convert_fusion.2 = bf16[8,2048]{1,0:T(8,128)(2,1)S(1)} fusion(bf16[8,2048]{1,0:T(8,128)(2,1)S(1)} %copy-done.3, bf16[2048,2048]{1,0:T(8,128)(2,1)} %param.26), kind=kOutput, calls=%fused_computation.7 | convolution fusion | flops 67125248 | bytes 8454144 | tf_op jit(solution)/shard_map/dot_general | solution.py:149
  22.3 4.0 %copy.82 = bf16[8,1024,128]{1,2,0:T(8,128)(2,1)} copy(bf16[8,1024,128]{2,1,0:T(8,128)(2,1)} %param.22) | data formatting | bytes 4194304 | tf_op args[1]
  26.5 1.3 gather_fusion
  28.1 2.2 %fusion.47 = (f32[8,2,16]{2,1,0:T(2,128)S(1)}, f32[8,2,16,1024]{3,2,1,0:T(8,128)S(1)}) fusion(f32[8,2,1024]{2,1,0:T(2,128)S(1)} %add_bitcast_fusion, bf16[8,2,16,64]{3,2,1,0:T(8,128)(2,1)} %copy-done.7, bf16[8,1024,2,64]{1,3,2,0:T(8,128)(2,1)} %bitcast.113, pred[8,1024]{1,0:T(8,128)(4,1)S(1)} %iota_compare_fusion), kind=kOutput, calls=%fused_computation.123 | convolution fusion | flops 34602752 | bytes 3253248 | tf_op jit(solution)/shard_map/bkgd,blkd->bkgl/dot_general | solution.py:61
  30.9 3.0 %fusion.8 = bf16[8,2,16,64]{3,2,1,0:T(8,128)(2,1)} fusion(bf16[8,1024,2,64]{1,3,2,0:T(8,128)(2,1)} %bitcast.129, f32[8,2,16,1024]{3,2,1,0:T(8,128)S(1)} %get-tuple-element.32, f32[8,2,16]{2,1,0:T(2,128)S(1)} %get-tuple-element.26, f32[8,2,16]{2,1,0:T(2,128)S(1)} %multiply_maximum_fusion, f32[8,2,64]{2,1,0:T(2,128)S(1)} %reshape.216, ...), kind=kOutput, calls=%fused_computation.21 | convolution fusion | flops 34390016 | bytes 3185664 | tf_op jit(solution)/shard_map/bkgl,blkd->bkgd/dot_general | solution.py:79
  33.9 1.0 convert_element_type.102
  34.9 0.9 all_to_all.32
  35.8 4.3 %all-to-all-start = ((bf16[8,8,256]{2,1,0:T(8,128)(2,1)}), bf16[8,8,256]{2,1,0:T(8,128)(2,1)S(1)}, u32[]{:S(2)}, u32[]{:S(2)}) async-start(bf16[8,8,256]{2,1,0:T(8,128)(2,1)} %all_to_all.32), calls=%async_computation | async-start | bytes 65536 | tf_op jit(solution)/shard_map/all_to_all | solution.py:33
  40.1 1.4 fusion.46
  41.5 1.4 fusion.45
  45.5 2.0 %tile.2 = bf16[16,16,2048]{2,1,0:T(8,128)(2,1)} broadcast(bf16[16,2048]{1,0:T(8,128)(2,1)} %param.30), dimensions={1,2} | broadcast | bytes 1114112 | tf_op jit(solution)/shard_map/tile | solution.py:145
  47.5 6.0 %all-to-all-start.1 = ((bf16[16,16,2048]{2,1,0:T(8,128)(2,1)}), bf16[16,16,2048]{2,1,0:T(8,128)(2,1)S(1)}, u32[]{:S(2)}, u32[]{:S(2)}) async-start(bf16[16,16,2048]{2,1,0:T(8,128)(2,1)} %tile.2), calls=%async_computation.1 | async-start | bytes 2097152 | tf_op jit(solution)/shard_map/all_to_all | solution.py:33
  53.5 1.3 fusion.30
  55.4 1.3 copy.87
  56.8 1.3 convert_convert_fusion
  58.1 1.0 slice.69
  59.1 2.0 %collective-permute-start.4 = (bf16[72,2048]{1,0:T(8,128)(2,1)S(1)}, bf16[72,2048]{1,0:T(8,128)(2,1)S(1)}, u32[]{:S(2)}, u32[]{:S(2)}) collective-permute-start(bf16[72,2048]{1,0:T(8,128)(2,1)S(1)} %slice.69), channel_id=1, source_target_pairs={{0,32},{1,33},{2,34},{3,35},{4,36},{5,37},{6,38},{7,39},{8,40},{9,... | collective-permute-start | bytes 884744 | tf_op jit(solution)/shard_map/ppermute | solution.py:25
  61.8 1.3 collective-permute-start.5
  63.1 2.3 %constant_dynamic-update-slice_fusion.5 = (bf16[576,2048]{1,0:T(8,128)(2,1)}, bf16[1152,2048]{1,0:T(8,128)(2,1)}) fusion(bf16[576,2048]{1,0:T(8,128)(2,1)} %get-tuple-element.16, bf16[144,2048]{1,0:T(8,128)(2,1)} %collective-permute-done.2, bf16[1152,2048]{1,0:T(8,128)(2,1)} %get-tuple-element.17), kind=kLoop, calls=%fused_computation.55 | loop fusion | bytes 1769472
  65.4 1.2 constant_dynamic-update-slice_fusion.4
  66.6 8.8 %collective-permute-done.4 = bf16[72,2048]{1,0:T(8,128)(2,1)S(1)} collective-permute-done((bf16[72,2048]{1,0:T(8,128)(2,1)S(1)}, bf16[72,2048]{1,0:T(8,128)(2,1)S(1)}, u32[]{:S(2)}, u32[]{:S(2)}) %collective-permute-start.4) | collective-permute-done | bytes 294944 | tf_op jit(solution)/shard_map/ppermute | solution.py:25
  75.4 0.9 constant_dynamic-update-slice_fusion.3
  76.3 1.0 fusion
  77.3 4.4 %all-to-all-start.2 = ((bf16[8,8,2048]{2,1,0:T(8,128)(2,1)}), bf16[8,8,2048]{2,1,0:T(8,128)(2,1)S(1)}, u32[]{:S(2)}, u32[]{:S(2)}) async-start(bf16[8,8,2048]{2,1,0:T(8,128)(2,1)} %fusion), calls=%async_computation.2 | async-start | bytes 524288 | tf_op jit(solution)/shard_map/all_to_all | solution.py:33
  81.7 1.8 %constant_dynamic-update-slice_fusion.2 = (bf16[576,2048]{1,0:T(8,128)(2,1)}, bf16[1152,2048]{1,0:T(8,128)(2,1)}) fusion(bf16[576,2048]{1,0:T(8,128)(2,1)} %get-tuple-element.14, bf16[72,2048]{1,0:T(8,128)(2,1)} %collective-permute-done.5, bf16[1152,2048]{1,0:T(8,128)(2,1)} %get-tuple-element.15), kind=kLoop, calls=%fused_computation.52 | loop fusion | bytes 884736 | tf_op jit(solution)/shard_map/concatenate | solution.py:114
  84.0 5.2 %all-to-all-done.2 = bf16[8,8,2048]{2,1,0:T(8,128)(2,1)S(1)} async-done(((bf16[8,8,2048]{2,1,0:T(8,128)(2,1)}), bf16[8,8,2048]{2,1,0:T(8,128)(2,1)S(1)}, u32[]{:S(2)}, u32[]{:S(2)}) %all-to-all-start.2) | async-done | bytes 262176 | tf_op jit(solution)/shard_map/all_to_all | solution.py:33
  90.0 26.9 %all_to_all.48 = bf16[64,8,1280]{2,1,0:T(8,128)(2,1)S(1)} all-to-all(bf16[64,8,1280]{2,1,0:T(8,128)(2,1)S(1)} %bitcast.120), channel_id=1, replica_groups={{0,2,4,6,8,10,12,14,16,18,20,22,24,26,28,30,32,34,36,38,40,42,44,46,48,..., dimensions={0} | all-to-all | bytes 2621440 | tf_op jit(solution)/shard_map/all_to_all | solution.py:33
  117.6 0.9 copy.98
  118.7 3.5 %constant_dynamic-update-slice_fusion.9 = bf16[1152,2048]{1,0:T(8,128)(2,1)} fusion(bf16[1152,2048]{1,0:T(8,128)(2,1)} %get-tuple-element.13, bf16[576,2048]{1,0:T(8,128)(2,1)} %collective-permute-done.6), kind=kLoop, calls=%fused_computation.59 | loop fusion | bytes 4718592 | tf_op jit(solution)/shard_map/concatenate | solution.py:115
  122.2 2.1 %fusion.52 = f32[384,448]{0,1:T(8,128)} fusion(bf16[384,2048]{1,0:T(8,128)(2,1)S(1)} %constant_dynamic-update-slice_fusion, bf16[2048,448]{0,1:T(8,128)(2,1)S(1)} %copy-done.17), kind=kOutput, calls=%fused_computation.127 | convolution fusion | flops 704643072 | bytes 4096000 | tf_op jit(solution)/shard_map/dot_general | solution.py:201
  124.3 5.4 %fusion.13 = f32[384,2048]{1,0:T(8,128)} fusion(bf16[448,2048]{1,0:T(8,128)(2,1)S(1)} %copy-done, f32[384,448]{0,1:T(8,128)} %fusion.52, bf16[384,2048]{1,0:T(8,128)(2,1)S(1)} %constant_dynamic-update-slice_fusion, bf16[2048,448]{0,1:T(8,128)(2,1)} %param.38), kind=kOutput, calls=%fused_computation.35 | convolution fusion | flops 1410318336 | bytes 9076736 | tf_op jit(solution)/shard_map/dot_general | solution.py:204
  129.7 2.4 %slice.84 = bf16[192,2048]{1,0:T(8,128)(2,1)} slice(f32[384,2048]{1,0:T(8,128)} %fusion.13), slice={[192:384], [0:2048]} | slice | bytes 1572864 | tf_op jit(solution)/shard_map/slice | solution.py:206
  132.6 4.2 %fusion.44 = (bf16[8,1,48,2048]{3,2,1,0:T(8,128)(2,1)S(1)}, bf16[8,1,48,2048]{3,2,1,0:T(8,128)(2,1)S(1)}, bf16[8,1,48,2048]{3,2,1,0:T(8,128)(2,1)}) fusion(bf16[8,3,48,2048]{3,2,1,0:T(8,128)(2,1)} %bitcast.28), kind=kLoop, calls=%fused_computation.120 | loop fusion | bytes 9437184 | tf_op jit(solution)/shard_map/slice | solution.py:117
  136.8 1.3 fusion.53
  138.1 3.6 %convolution_convert_fusion = bf16[128,2048]{1,0:T(8,128)(2,1)} fusion(bf16[384,2048]{1,0:T(8,128)(2,1)S(1)} %bitcast.114, bf16[128,2048]{1,0:T(8,128)(2,1)} %bitcast.123, bf16[384,2048]{1,0:T(8,128)(2,1)} %bitcast.115, f32[128,384]{1,0:T(8,128)} %fusion.53), kind=kOutput, calls=%fused_computation.1 | convolution fusion | flops 403210240 | bytes 4390912 | tf_op jit(solution)/shard_map/dot_general | solution.py:199
  141.7 1.8 %fusion.3 = bf16[192,2048]{1,0:T(8,128)(2,1)S(1)} fusion(f32[384,2048]{1,0:T(8,128)} %fusion.13, bf16[192,2048]{1,0:T(8,128)(2,1)} %collective-permute-done.1), kind=kLoop, calls=%fused_computation.10 | loop fusion | flops 1179648 | bytes 3145728 | tf_op jit(solution)/shard_map/convert.2
  144.1 1.2 copy.92
  145.3 4.8 %all-to-all-start.4 = ((bf16[64,8,1280]{2,1,0:T(8,128)(2,1)}), bf16[64,8,1280]{2,1,0:T(8,128)(2,1)S(1)}, u32[]{:S(2)}, u32[]{:S(2)}) async-start(bf16[64,8,1280]{2,1,0:T(8,128)(2,1)} %bitcast.33), calls=%async_computation.4 | async-start | bytes 2621440 | tf_op jit(solution)/shard_map/all_to_all | solution.py:33
  150.1 0.8 constant_dynamic-slice_fusion
  151.0 21.1 %all-to-all-done.4 = bf16[64,8,1280]{2,1,0:T(8,128)(2,1)S(1)} async-done(((bf16[64,8,1280]{2,1,0:T(8,128)(2,1)}), bf16[64,8,1280]{2,1,0:T(8,128)(2,1)S(1)}, u32[]{:S(2)}, u32[]{:S(2)}) %all-to-all-start.4) | async-done | bytes 1310752 | tf_op jit(solution)/shard_map/all_to_all | solution.py:33
  (108 shorter events, 11.0 us)
Async XLA Ops:
  0.0 124.3 %copy-start = (bf16[448,2048]{1,0:T(8,128)(2,1)S(1)}, bf16[448,2048]{1,0:T(8,128)(2,1)}, u32[]{:S(2)}) copy-start(bf16[448,2048]{1,0:T(8,128)(2,1)} %param.39) | copy-start | bytes 5505028
  0.0 10.4 %copy-start.16 = (s32[8]{0:T(128)S(1)}, s32[8]{0:T(128)}, u32[]{:S(2)}) copy-start(s32[8]{0:T(128)} %param.25) | copy-start | bytes 100
  6.3 51.8 %collective-permute-start.2 = (bf16[144,2048]{1,0:T(8,128)(2,1)}, bf16[144,2048]{1,0:T(8,128)(2,1)}, u32[]{:S(2)}, u32[]{:S(2)}) collective-permute-start(bf16[144,2048]{1,0:T(8,128)(2,1)} %pad_maximum_fusion.1), channel_id=1, source_target_pairs={{0,32},{1,33},{2,34},{3,35},{4,36},{5,37},{6,38},{7,39},{8,40},{9,... | collective-permute-start | bytes 1769480 | tf_op jit(solution)/shard_map/ppermute | solution.py:25
  8.3 52.8 %collective-permute-start.3 = (bf16[144,2048]{1,0:T(8,128)(2,1)}, bf16[144,2048]{1,0:T(8,128)(2,1)S(1)}, u32[]{:S(2)}, u32[]{:S(2)}) collective-permute-start(bf16[144,2048]{1,0:T(8,128)(2,1)} %pad_maximum_fusion.1), channel_id=1, source_target_pairs={{0,96},{1,97},{2,98},{3,99},{4,100},{5,101},{6,102},{7,103},{8,104... | collective-permute-start | bytes 1769480 | tf_op jit(solution)/shard_map/ppermute | solution.py:25
  10.5 4.0 %copy-start.3 = (bf16[8,2048]{1,0:T(8,128)(2,1)S(1)}, bf16[8,2048]{1,0:T(8,128)(2,1)}, u32[]{:S(2)}) copy-start(bf16[8,2048]{1,0:T(8,128)(2,1)} %param.21) | copy-start | bytes 98308
  10.5 4.0 %copy-start.18 = (bf16[2048,2]{0,1:T(2,128)(2,1)S(1)}, bf16[2048,2]{0,1:T(2,128)(2,1)}, u32[]{:S(2)}) copy-start(bf16[2048,2]{0,1:T(2,128)(2,1)} %param.29) | copy-start | bytes 24580
  10.5 4.2 %copy-start.6 = (f32[8,1024,2]{1,2,0:T(2,128)S(1)}, f32[8,1024,2]{1,2,0:T(2,128)}, u32[]{:S(2)}) copy-start(f32[8,1024,2]{1,2,0:T(2,128)} %param.24) | copy-start | bytes 196612
  22.2 5.7 %copy-start.7 = (bf16[8,2,16,64]{3,2,1,0:T(8,128)(2,1)}, bf16[8,2,16,64]{3,2,1,0:T(8,128)(2,1)S(1)}, u32[]{:S(2)}) copy-start(bf16[8,2,16,64]{3,2,1,0:T(8,128)(2,1)S(1)} %reshape.203) | copy-start | bytes 98308
  22.2 4.0 %copy-start.4 = (bf16[2048,128]{1,0:T(8,128)(2,1)S(1)}, bf16[2048,128]{1,0:T(8,128)(2,1)}, u32[]{:S(2)}) copy-start(bf16[2048,128]{1,0:T(8,128)(2,1)} %param.27) | copy-start | bytes 1572868
  28.1 2.6 %copy-start.5 = (bf16[2048,128]{1,0:T(8,128)(2,1)S(1)}, bf16[2048,128]{1,0:T(8,128)(2,1)}, u32[]{:S(2)}) copy-start(bf16[2048,128]{1,0:T(8,128)(2,1)} %param.28) | copy-start | bytes 1572868
  35.8 9.7 %all-to-all-start = ((bf16[8,8,256]{2,1,0:T(8,128)(2,1)}), bf16[8,8,256]{2,1,0:T(8,128)(2,1)S(1)}, u32[]{:S(2)}, u32[]{:S(2)}) async-start(bf16[8,8,256]{2,1,0:T(8,128)(2,1)} %all_to_all.32), calls=%async_computation | async-start | bytes 65536 | tf_op jit(solution)/shard_map/all_to_all | solution.py:33
  43.6 0.5 copy-start.13
  47.5 28.8 %all-to-all-start.1 = ((bf16[16,16,2048]{2,1,0:T(8,128)(2,1)}), bf16[16,16,2048]{2,1,0:T(8,128)(2,1)S(1)}, u32[]{:S(2)}, u32[]{:S(2)}) async-start(bf16[16,16,2048]{2,1,0:T(8,128)(2,1)} %tile.2), calls=%async_computation.1 | async-start | bytes 2097152 | tf_op jit(solution)/shard_map/all_to_all | solution.py:33
  59.1 16.3 %collective-permute-start.4 = (bf16[72,2048]{1,0:T(8,128)(2,1)S(1)}, bf16[72,2048]{1,0:T(8,128)(2,1)S(1)}, u32[]{:S(2)}, u32[]{:S(2)}) collective-permute-start(bf16[72,2048]{1,0:T(8,128)(2,1)S(1)} %slice.69), channel_id=1, source_target_pairs={{0,32},{1,33},{2,34},{3,35},{4,36},{5,37},{6,38},{7,39},{8,40},{9,... | collective-permute-start | bytes 884744 | tf_op jit(solution)/shard_map/ppermute | solution.py:25
  61.8 19.9 %collective-permute-start.5 = (bf16[72,2048]{1,0:T(8,128)(2,1)}, bf16[72,2048]{1,0:T(8,128)(2,1)}, u32[]{:S(2)}, u32[]{:S(2)}) collective-permute-start(bf16[72,2048]{1,0:T(8,128)(2,1)} %slice.70), channel_id=1, source_target_pairs={{0,96},{1,97},{2,98},{3,99},{4,100},{5,101},{6,102},{7,103},{8,104... | collective-permute-start | bytes 884744 | tf_op jit(solution)/shard_map/ppermute | solution.py:25
  66.6 23.0 %copy-start.9 = (f32[1,2048]{1,0:T(1,128)S(1)}, f32[1,2048]{1,0:T(1,128)}, u32[]{:S(2)}) copy-start(f32[1,2048]{1,0:T(1,128)} %get-tuple-element.30) | copy-start | bytes 24580
  66.6 23.0 %copy-start.10 = (f32[1,2048]{1,0:T(1,128)S(1)}, f32[1,2048]{1,0:T(1,128)}, u32[]{:S(2)}) copy-start(f32[1,2048]{1,0:T(1,128)} %get-tuple-element.28) | copy-start | bytes 24580
  75.4 14.3 %copy-start.11 = (bf16[8,3,8]{2,0,1:T(8,128)(2,1)S(1)}, bf16[8,3,8]{2,0,1:T(8,128)(2,1)}, u32[]{:S(2)}) copy-start(bf16[8,3,8]{2,0,1:T(8,128)(2,1)} %convert_convert_fusion) | copy-start | bytes 1156
  75.4 14.3 %copy-start.12 = (bf16[8,2,8]{2,0,1:T(8,128)(2,1)S(1)}, bf16[8,2,8]{2,0,1:T(8,128)(2,1)}, u32[]{:S(2)}) copy-start(bf16[8,2,8]{2,0,1:T(8,128)(2,1)} %fusion.30) | copy-start | bytes 772
  77.3 11.9 %all-to-all-start.2 = ((bf16[8,8,2048]{2,1,0:T(8,128)(2,1)}), bf16[8,8,2048]{2,1,0:T(8,128)(2,1)S(1)}, u32[]{:S(2)}, u32[]{:S(2)}) async-start(bf16[8,8,2048]{2,1,0:T(8,128)(2,1)} %fusion), calls=%async_computation.2 | async-start | bytes 524288 | tf_op jit(solution)/shard_map/all_to_all | solution.py:33
  83.5 35.1 %collective-permute-start.6 = (bf16[576,2048]{1,0:T(8,128)(2,1)}, bf16[576,2048]{1,0:T(8,128)(2,1)}, u32[]{:S(2)}, u32[]{:S(2)}) collective-permute-start(bf16[576,2048]{1,0:T(8,128)(2,1)} %get-tuple-element.12), channel_id=1, source_target_pairs={{0,1},{1,0},{2,3},{3,2},{4,5},{5,4},{6,7},{7,6},{8,9},{9,8},{10,11... | collective-permute-start | bytes 7077896 | tf_op jit(solution)/shard_map/ppermute | solution.py:29
  117.3 4.9 %collective-permute-start = (bf16[192,2048]{1,0:T(8,128)(2,1)S(1)}, bf16[192,2048]{1,0:T(8,128)(2,1)S(1)}, u32[]{:S(2)}, u32[]{:S(2)}) collective-permute-start(bf16[192,2048]{1,0:T(8,128)(2,1)S(1)} %bitcast.126), channel_id=1, source_target_pairs={{0,1},{1,0},{2,3},{3,2},{4,5},{5,4},{6,7},{7,6},{8,9},{9,8},{10,11... | collective-permute-start | bytes 2359304 | tf_op jit(solution)/shard_map/ppermute | solution.py:29
  118.6 3.6 %copy-start.17 = (bf16[2048,448]{0,1:T(8,128)(2,1)S(1)}, bf16[2048,448]{0,1:T(8,128)(2,1)}, u32[]{:S(2)}) copy-start(bf16[2048,448]{0,1:T(8,128)(2,1)} %param.37) | copy-start | bytes 5505028
  132.1 9.6 %collective-permute-start.1 = (bf16[192,2048]{1,0:T(8,128)(2,1)}, bf16[192,2048]{1,0:T(8,128)(2,1)}, u32[]{:S(2)}, u32[]{:S(2)}) collective-permute-start(bf16[192,2048]{1,0:T(8,128)(2,1)} %slice.84), channel_id=1, source_target_pairs={{0,1},{1,0},{2,3},{3,2},{4,5},{5,4},{6,7},{7,6},{8,9},{9,8},{10,11... | collective-permute-start | bytes 2359304 | tf_op jit(solution)/shard_map/ppermute | solution.py:29
  132.6 4.2 %copy-start.1 = (bf16[16,8,8,256]{3,1,2,0:T(8,128)(2,1)S(1)}, bf16[16,8,8,256]{3,1,2,0:T(8,128)(2,1)}, u32[]{:S(2)}) copy-start(bf16[16,8,8,256]{3,1,2,0:T(8,128)(2,1)} %copy.98) | copy-start | bytes 1572868
  141.7 1.9 %copy-start.2 = (bf16[128,2048]{1,0:T(8,128)(2,1)S(1)}, bf16[128,2048]{1,0:T(8,128)(2,1)}, u32[]{:S(2)}) copy-start(bf16[128,2048]{1,0:T(8,128)(2,1)} %convolution_convert_fusion) | copy-start | bytes 1572868
  144.1 6.8 %copy-start.14 = (s32[8,2]{0,1:T(2,128)S(1)}, s32[8,2]{0,1:T(2,128)}, u32[]{:S(2)}) copy-start(s32[8,2]{0,1:T(2,128)} %copy-done.13) | copy-start | bytes 196
  145.3 26.8 %all-to-all-start.4 = ((bf16[64,8,1280]{2,1,0:T(8,128)(2,1)}), bf16[64,8,1280]{2,1,0:T(8,128)(2,1)S(1)}, u32[]{:S(2)}, u32[]{:S(2)}) async-start(bf16[64,8,1280]{2,1,0:T(8,128)(2,1)} %bitcast.33), calls=%async_computation.4 | async-start | bytes 2621440 | tf_op jit(solution)/shard_map/all_to_all | solution.py:33
  172.3 0.7 copy-start.15
  172.3 1.2 copy-start.8
